TPU v7x, 32 devices: a whole 2x2x4 slice. The times are simulated.
32 devices in a mesh: ra: 4 (over z), cb: 4 (over y, x), dp: 2 (over core).
Axes of the slice: x: 2, y: 2, z: 4, core: 2. Of those that a mesh axis runs over, the one named last changes fastest.
Arguments:
- tokens: bfloat16 [512, 4096], P('dp', 'ra'), may hold values from -6 to 6, as said below
- pre_gain_first: bfloat16 [4096], P('ra'), may hold values from 0.099609375 to 1.8984375
- gate_first: bfloat16 [4096, 11264], P('ra', 'cb'), may hold values from -0.1875 to 0.1875
- up_first: bfloat16 [4096, 11264], P('ra', 'cb'), may hold values from -0.09375 to 0.09375
- down_first: bfloat16 [11264, 4096], P('cb', 'ra'), may hold values from -1 to 1, as said below
- post_gain_first: bfloat16 [4096], P('ra'), may hold values from 0.099609375 to 1.8984375
- pre_gain_second: bfloat16 [4096], P('ra'), may hold values from 0.099609375 to 1.8984375
- gate_second: bfloat16 [4096, 11264], P('ra', 'cb'), may hold values from -0.1875 to 0.1875
- up_second: bfloat16 [4096, 11264], P('ra', 'cb'), may hold values from -0.09375 to 0.09375
- down_second: bfloat16 [11264, 4096], P('cb', 'ra'), may hold values from -1 to 1, as said below
- post_gain_second: bfloat16 [4096], P('ra'), may hold values from 0.099609375 to 1.8984375
Outputs:
- stream_out: float32 [512, 4096], P('dp', 'ra')
Inputs may be any that keep to these rules, and one draw needn't show every extreme that they name: tokens: real-valued activations; groups of 256 consecutive features carry different scales, and tokens different scales. down_first: real-valued weights; groups of 256 consecutive columns carry different scales. down_second: real-valued weights; groups of 256 consecutive columns carry different scales.
All inputs are finite; a program needn't handle non-finite values.
Results may differ from a plain program's by a relative error of at most 0.034.
Values may be sent and summed in bfloat16 or wider, within the bound.
A program may use at most 128 MiB of HBM per device.

v0:
```python
import jax
import jax.numpy as jnp
from jax import lax
from jax.sharding import PartitionSpec as P

D = 4096


EPS = 1e-06


def stream_squares(stream):
    return lax.psum(jnp.sum(stream * stream, axis=1, keepdims=True), "ra")


def branch_squares(branch):
    return lax.psum(jnp.sum(branch * branch, axis=1, keepdims=True), "ra")


def project(stream, squares, pre_gain, gate_weight, up_weight, down_weight):
    normed = (stream * lax.rsqrt(squares / D + EPS) * pre_gain.astype(jnp.float32)).astype(
        jnp.bfloat16
    )
    gate_part = jnp.dot(normed, gate_weight, preferred_element_type=jnp.float32)
    up_part = jnp.dot(normed, up_weight, preferred_element_type=jnp.float32)
    gate, up = (
        lax.psum_scatter(
            gate_part.astype(jnp.bfloat16), "ra", scatter_dimension=0, tiled=True
        ).astype(jnp.float32),
        lax.psum_scatter(
            up_part.astype(jnp.bfloat16), "ra", scatter_dimension=0, tiled=True
        ).astype(jnp.float32),
    )
    share = (jax.nn.silu(gate) * up).astype(jnp.bfloat16)
    hidden = lax.all_gather(share, "ra", axis=0, tiled=True)
    partial_value = jnp.dot(hidden, down_weight, preferred_element_type=jnp.float32)
    total = lax.psum(partial_value.astype(jnp.bfloat16), "cb")
    return total.astype(jnp.float32)


def shards(
    tokens,
    pre_gain_first,
    gate_first,
    up_first,
    down_first,
    post_gain_first,
    pre_gain_second,
    gate_second,
    up_second,
    down_second,
    post_gain_second,
):
    stream = tokens.astype(jnp.float32)
    squares = stream_squares(stream)
    branch = project(stream, squares, pre_gain_first, gate_first, up_first, down_first)
    own_sq = branch_squares(branch)
    stream = stream + 0.5 * branch * lax.rsqrt(own_sq / D + EPS) * post_gain_first.astype(
        jnp.float32
    )
    squares = stream_squares(stream)
    branch = project(stream, squares, pre_gain_second, gate_second, up_second, down_second)
    own_sq = branch_squares(branch)
    stream = stream + 0.5 * branch * lax.rsqrt(own_sq / D + EPS) * post_gain_second.astype(
        jnp.float32
    )
    return stream


def solution(mesh):
    placed = (
        P("dp", "ra"),
        P("ra"),
        P("ra", "cb"),
        P("ra", "cb"),
        P("cb", "ra"),
        P("ra"),
        P("ra"),
        P("ra", "cb"),
        P("ra", "cb"),
        P("cb", "ra"),
        P("ra"),
    )
    return jax.shard_map(
        shards, mesh=mesh, in_specs=placed, out_specs=P("dp", "ra"), check_vma=False
    )
```

profile of v0, /device:TPU:0, one launch (start us, length us, event | category | flops | bytes accessed | tf_op | source)
XLA Modules:
  0.0 383.0 jit_solution(4912971013089754549)
XLA Ops:
  6.5 0.7 convert_element_type.64
  7.2 1.3 fusion.5
  8.5 13.5 %psum.42 = f32[256,1]{0,1:T(1,128)S(1)} all-reduce(f32[256,1]{0,1:T(1,128)S(1)} %bitcast.21), channel_id=1, replica_groups=mesh['ra'=4,'cb'=4,'dp'=2] {'ra'}, use_global_device_ids=true, to_apply=%region_1.0 | all-reduce | flops 256 | bytes 2048 | tf_op jit(solution)/shard_map/psum | solution.py:13
  22.0 5.7 %convolution_convert_fusion.3 = bf16[256,2816]{1,0:T(8,128)(2,1)} fusion(bf16[1024,2816]{1,0:T(8,128)(2,1)} %param.13, bf16[256,1024]{1,0:T(8,128)(2,1)} %param.11, f32[1024]{0:T(1024)S(1)} %convert_element_type.64, f32[256]{0:T(256)S(1)} %bitcast.25), kind=kOutput, calls=%fused_computation.3 | convolution fusion | flops 1478164480 | bytes 7738368 | tf_op jit(solution)/shard_map/dot_general | solution.py:24
  27.7 0.0 reduce-scatter.7.cloned.1.call-start
  27.8 5.5 %convolution_convert_fusion.2 = bf16[256,2816]{1,0:T(8,128)(2,1)} fusion(bf16[1024,2816]{1,0:T(8,128)(2,1)} %param.14, bf16[256,1024]{1,0:T(8,128)(2,1)S(1)} %copy-done, f32[1024]{0:T(1024)S(1)} %convert_element_type.64, f32[256]{0:T(256)S(1)} %bitcast.26), kind=kOutput, calls=%fused_computation.2 | convolution fusion | flops 1478164480 | bytes 7738368 | tf_op jit(solution)/shard_map/dot_general | solution.py:25
  33.3 0.0 all-gather.3.cloned.1.call-start
  33.3 26.1 %reduce-scatter.5.cloned.1.call-done = bf16[64,2816]{1,0:T(8,128)(2,1)} async-done(((bf16[256,2816]{1,0:T(8,128)(2,1)}), bf16[64,2816]{1,0:T(8,128)(2,1)}) %reduce-scatter.5.cloned.1.call-update) | async-done | bytes 360464 | tf_op jit(solution)/shard_map/reduce_scatter | solution.py:27
  59.5 34.5 %reduce-scatter.7.cloned.1.call-done = bf16[64,2816]{1,0:T(8,128)(2,1)} async-done(((bf16[256,2816]{1,0:T(8,128)(2,1)}), bf16[64,2816]{1,0:T(8,128)(2,1)}) %reduce-scatter.7.cloned.1.call-update) | async-done | bytes 360464 | tf_op jit(solution)/shard_map/reduce_scatter | solution.py:30
  94.0 2.0 fusion.17
  96.1 0.0 all-reduce.3.cloned.1.call-start
  96.1 33.6 %all-gather.3.cloned.1.call-done = bf16[256,2816]{1,0:T(8,128)(2,1)} async-done(((bf16[64,2816]{1,0:T(8,128)(2,1)}), bf16[256,2816]{1,0:T(8,128)(2,1)}) %all-gather.3.cloned.1.call-update) | async-done | bytes 1441808 | tf_op jit(solution)/shard_map/all_gather | solution.py:35
  129.7 5.5 %convolution_convert_fusion.5 = bf16[256,1024]{1,0:T(8,128)(2,1)} fusion(bf16[256,2816]{1,0:T(8,128)(2,1)} %all-gather.3.cloned.1.call-done, bf16[2816,1024]{1,0:T(8,128)(2,1)} %param.15), kind=kOutput, calls=%fused_computation.12 | convolution fusion | flops 1476657152 | bytes 7733248 | tf_op jit(solution)/shard_map/dot_general | solution.py:36
  135.3 0.0 reduce-scatter.9.cloned.1.call-start
  135.4 44.4 %all-reduce.3.cloned.1.call-done = bf16[256,1024]{1,0:T(8,128)(2,1)} async-done(((bf16[256,1024]{1,0:T(8,128)(2,1)}), bf16[256,1024]{1,0:T(8,128)(2,1)}) %all-reduce.3.cloned.1.call-update) | async-done | bytes 524304 | tf_op jit(solution)/shard_map/psum | solution.py:37
  179.8 1.2 fusion
  181.0 11.7 %psum.44 = f32[256,1]{0,1:T(1,128)S(1)} all-reduce(f32[256,1]{0,1:T(1,128)S(1)} %bitcast.22), channel_id=1, replica_groups=mesh['ra'=4,'cb'=4,'dp'=2] {'ra'}, use_global_device_ids=true, to_apply=%region_6.7 | all-reduce | flops 256 | bytes 2048 | tf_op jit(solution)/shard_map/psum | solution.py:17
  192.7 1.4 multiply_reduce_fusion
  194.2 8.4 %psum.45 = f32[256,1]{0,1:T(1,128)S(1)} all-reduce(f32[256,1]{0,1:T(1,128)S(1)} %bitcast.24), channel_id=1, replica_groups=mesh['ra'=4,'cb'=4,'dp'=2] {'ra'}, use_global_device_ids=true, to_apply=%region_8.9 | all-reduce | flops 256 | bytes 2048 | tf_op jit(solution)/shard_map/psum | solution.py:13
  202.6 5.8 %convolution_convert_fusion.1 = bf16[256,2816]{1,0:T(8,128)(2,1)} fusion(bf16[1024,2816]{1,0:T(8,128)(2,1)} %param.18, bf16[256,1024]{1,0:T(8,128)(2,1)} %all-reduce.3.cloned.1.call-done, bf16[256,1024]{1,0:T(8,128)(2,1)S(1)} %copy-done, f32[1024]{0:T(1024)S(1)} %convert_element_type.74, f32[256]{0:T(256)S(1)} %bitcast.27, ...), kind=kOutput, calls=%fused_computation.1 | convolution fusion | flops 1479213056 | bytes 8267776 | tf_op jit(solution)/shard_map/dot_general | solution.py:24
  208.4 0.0 reduce-scatter.11.cloned.1.call-start
  208.5 5.6 %convolution_convert_fusion = bf16[256,2816]{1,0:T(8,128)(2,1)} fusion(bf16[1024,2816]{1,0:T(8,128)(2,1)} %param.19, bf16[256,1024]{1,0:T(8,128)(2,1)S(1)} %copy-done.1, bf16[256,1024]{1,0:T(8,128)(2,1)S(1)} %copy-done, f32[1024]{0:T(1024)S(1)} %convert_element_type.74, f32[256]{0:T(256)S(1)} %bitcast.28, f32[1024]{0:T(1024)S(1)} %convert_element_type.73, ...), kind=kOutput, calls=%fused_computation | convolution fusion | flops 1479213056 | bytes 8267776 | tf_op jit(solution)/shard_map/dot_general | solution.py:25
  214.1 0.0 all-gather.5.cloned.1.call-start
  214.1 26.5 %reduce-scatter.9.cloned.1.call-done = bf16[64,2816]{1,0:T(8,128)(2,1)} async-done(((bf16[256,2816]{1,0:T(8,128)(2,1)}), bf16[64,2816]{1,0:T(8,128)(2,1)}) %reduce-scatter.9.cloned.1.call-update) | async-done | bytes 360464 | tf_op jit(solution)/shard_map/reduce_scatter | solution.py:27
  240.6 34.4 %reduce-scatter.11.cloned.1.call-done = bf16[64,2816]{1,0:T(8,128)(2,1)} async-done(((bf16[256,2816]{1,0:T(8,128)(2,1)}), bf16[64,2816]{1,0:T(8,128)(2,1)}) %reduce-scatter.11.cloned.1.call-update) | async-done | bytes 360464 | tf_op jit(solution)/shard_map/reduce_scatter | solution.py:30
  275.0 2.0 fusion.16
  277.1 33.6 %all-gather.5.cloned.1.call-done = bf16[256,2816]{1,0:T(8,128)(2,1)} async-done(((bf16[64,2816]{1,0:T(8,128)(2,1)}), bf16[256,2816]{1,0:T(8,128)(2,1)}) %all-gather.5.cloned.1.call-update) | async-done | bytes 1441808 | tf_op jit(solution)/shard_map/all_gather | solution.py:35
  310.8 5.5 %convolution_convert_fusion.4 = bf16[256,1024]{1,0:T(8,128)(2,1)} fusion(bf16[256,2816]{1,0:T(8,128)(2,1)} %all-gather.5.cloned.1.call-done, bf16[2816,1024]{1,0:T(8,128)(2,1)} %param.20), kind=kOutput, calls=%fused_computation.11 | convolution fusion | flops 1476657152 | bytes 7733248 | tf_op jit(solution)/shard_map/dot_general | solution.py:36
  316.3 44.5 %all-reduce.5.cloned.1.call-done = bf16[256,1024]{1,0:T(8,128)(2,1)} async-done(((bf16[256,1024]{1,0:T(8,128)(2,1)}), bf16[256,1024]{1,0:T(8,128)(2,1)}) %all-reduce.5.cloned.1.call-update) | async-done | bytes 524304 | tf_op jit(solution)/shard_map/psum | solution.py:37
  360.8 1.2 fusion.2
  362.1 11.7 %psum.47 = f32[256,1]{0,1:T(1,128)S(1)} all-reduce(f32[256,1]{0,1:T(1,128)S(1)} %bitcast.23), channel_id=1, replica_groups=mesh['ra'=4,'cb'=4,'dp'=2] {'ra'}, use_global_device_ids=true, to_apply=%region_13.14 | all-reduce | flops 256 | bytes 2048 | tf_op jit(solution)/shard_map/psum | solution.py:17
  373.8 2.4 fusion.4
  (27 shorter events, 0.3 us)
Async XLA Ops:
  6.5 52.9 %reduce-scatter.5.cloned.1.call-start = ((), (), s32[]{:S(2)}) async-start(), calls=%async_computation.4 | async-start | bytes 1802240 | tf_op jit(solution)/shard_map/reduce_scatter | solution.py:27
  7.2 20.5 %copy-start = (bf16[256,1024]{1,0:T(8,128)(2,1)S(1)}, bf16[256,1024]{1,0:T(8,128)(2,1)}, u32[]{:S(2)}) copy-start(bf16[256,1024]{1,0:T(8,128)(2,1)} %param.11) | copy-start | bytes 1572868
  27.7 66.3 %reduce-scatter.7.cloned.1.call-start = ((), (), s32[]{:S(2)}) async-start(), calls=%async_computation.5 | async-start | bytes 1802240 | tf_op jit(solution)/shard_map/reduce_scatter | solution.py:30
  33.3 96.5 %all-gather.3.cloned.1.call-start = ((), (), s32[]{:S(2)}) async-start(), calls=%async_computation.6 | async-start | bytes 1802240 | tf_op jit(solution)/shard_map/all_gather | solution.py:35
  96.1 39.3 %copy-start.2 = (bf16[1024]{0:T(1024)(128)(2,1)S(1)}, bf16[1024]{0:T(1024)(128)(2,1)}, u32[]{:S(2)}) copy-start(bf16[1024]{0:T(1024)(128)(2,1)} %param.16) | copy-start | bytes 6148
  96.1 39.3 %copy-start.3 = (bf16[1024]{0:T(1024)(128)(2,1)S(1)}, bf16[1024]{0:T(1024)(128)(2,1)}, u32[]{:S(2)}) copy-start(bf16[1024]{0:T(1024)(128)(2,1)} %param.17) | copy-start | bytes 6148
  96.1 83.7 %all-reduce.3.cloned.1.call-start = ((), (), s32[]{:S(2)}) async-start(), calls=%async_computation.7 | async-start | bytes 1048576 | tf_op jit(solution)/shard_map/psum | solution.py:37
  135.3 105.3 %reduce-scatter.9.cloned.1.call-start = ((), (), s32[]{:S(2)}) async-start(), calls=%async_computation.8 | async-start | bytes 1802240 | tf_op jit(solution)/shard_map/reduce_scatter | solution.py:27
  202.6 5.9 %copy-start.1 = (bf16[256,1024]{1,0:T(8,128)(2,1)S(1)}, bf16[256,1024]{1,0:T(8,128)(2,1)}, u32[]{:S(2)}) copy-start(bf16[256,1024]{1,0:T(8,128)(2,1)} %all-reduce.3.cloned.1.call-done) | copy-start | bytes 1572868
  208.4 66.6 %reduce-scatter.11.cloned.1.call-start = ((), (), s32[]{:S(2)}) async-start(), calls=%async_computation.9 | async-start | bytes 1802240 | tf_op jit(solution)/shard_map/reduce_scatter | solution.py:30
  214.1 96.7 %all-gather.5.cloned.1.call-start = ((), (), s32[]{:S(2)}) async-start(), calls=%async_computation.10 | async-start | bytes 1802240 | tf_op jit(solution)/shard_map/all_gather | solution.py:35
  277.1 39.3 %copy-start.4 = (bf16[1024]{0:T(1024)(128)(2,1)S(1)}, bf16[1024]{0:T(1024)(128)(2,1)}, u32[]{:S(2)}) copy-start(bf16[1024]{0:T(1024)(128)(2,1)} %param.21) | copy-start | bytes 6148
  277.1 83.8 %all-reduce.5.cloned.1.call-start = ((), (), s32[]{:S(2)}) async-start(), calls=%async_computation.11 | async-start | bytes 1048576 | tf_op jit(solution)/shard_map/psum | solution.py:37
Sparse Core Ops, SparseCore 0:
  27.8 31.5 reduce-scatter.4
  61.8 32.1 reduce-scatter.6
  96.2 33.5 all-gather.2
  135.4 44.3 all-reduce.2
  208.5 32.0 reduce-scatter.8
  242.8 32.1 reduce-scatter.10
  277.2 33.5 all-gather.4
  316.4 44.3 all-reduce.4
where the time goes:
time: 384 us; the launch traced here: 383 us
  waiting for transfers between devices  278 us (72%)
  blocking collectives  45.2 us (12%)
  matrix products  33.6 us (9%)
  between operations  13.6 us (4%)
  other arithmetic  12.4 us (3%)
    psum x2, waiting for transfers between devices, project(): total = lax.psum(partial_value.astype(jnp.bfloat16), 'cb')  88.9 us
    reduce_scatter x2, waiting for transfers between devices, project(): lax.psum_scatter(up_part.astype(jnp.bfloat16), 'ra', scatter_dimension=0,...  68.9 us
    all_gather x2, waiting for transfers between devices, project(): hidden = lax.all_gather(share, 'ra', axis=0, tiled=True)  67.2 us
    reduce_scatter x2, waiting for transfers between devices, project(): lax.psum_scatter(gate_part.astype(jnp.bfloat16), 'ra', scatter_dimension=...  52.7 us
    psum x2, blocking collectives, branch_squares(): return lax.psum(jnp.sum(branch * branch, axis=1, keepdims=True), 'ra')  23.4 us
    psum x2, blocking collectives, stream_squares(): return lax.psum(jnp.sum(stream * stream, axis=1, keepdims=True), 'ra')  21.9 us
    dot_general x2, matrix products, project(): gate_part = jnp.dot(normed, gate_weight, preferred_element_type=jnp.float32)  11.5 us
    dot_general x2, matrix products, project(): jnp.dot(hidden, down_weight, preferred_element_type=jnp.float32)  11.1 us
  transfers between devices with their start and end apart: 8, of which 8 were waited for; matrix products, arithmetic and copies ran while one was open for 3% of the time, Pallas kernels for 0%

commit v1 on v0

v1 whole, which is shorter than its diff:
```python
import functools

import jax
import jax.numpy as jnp
from jax import lax
from jax.experimental import pallas as pl
from jax.experimental.pallas import tpu as pltpu
from jax.sharding import PartitionSpec as P

EPS = 1e-06
MESH = pl.DeviceIdType.MESH
F32 = jnp.float32
BF16 = jnp.bfloat16
GROUPS = 2
SLICE = 256
LAG = 2
GAP = 3 * LAG


def dot(a, b):
    return jnp.dot(a, b, preferred_element_type=F32)


def kernel(
    n_ra, tokens, g_pre0, gate0, up0, down0, g_post0, g_pre1, gate1, up1, down1, g_post1,
    out, wgu, wd, pslot, hslot, pbuf, xbuf, ybuf, acc, branch, v1, r1, v2, r2,
    stats, sst, rss, gpre, gpost,
    w_sem, p_send, p_recv, h_send, h_recv, a_send, a_recv, st_send, st_recv, ss_send, ss_recv,
):
    rows, dl = xbuf.shape
    depth = dl * n_ra
    n_k = gate0.shape[1] // SLICE
    part_rows = rows // (2 * GROUPS)
    per_layer = GROUPS * n_k
    top = n_ra - 1
    span = LAG * top
    base = n_k + 2 * span + GAP
    base = max(base, per_layer)
    half = dl // 2

    z = lax.axis_index("ra")
    c = lax.axis_index("cb")
    x_nb = c + 1 - 2 * (c % 2)
    y_nb = c + 2 - 4 * (c // 2)

    def weight_copies(i):
        layer, k = divmod(i, n_k)
        gate, up, down = ((gate0, up0, down0), (gate1, up1, down1))[layer]
        cols = pl.ds(k * SLICE, SLICE)
        return (
            pltpu.make_async_copy(gate.at[:, cols], wgu.at[i, :, pl.ds(0, SLICE)], w_sem.at[i, 0]),
            pltpu.make_async_copy(up.at[:, cols], wgu.at[i, :, pl.ds(SLICE, SLICE)], w_sem.at[i, 1]),
            pltpu.make_async_copy(down.at[cols, :], wd.at[i], w_sem.at[i, 2]),
        )

    for i in range(2 * n_k):
        for copy in weight_copies(i):
            copy.start()

    barrier = pltpu.get_barrier_semaphore()
    for j in range(1, n_ra):
        pl.semaphore_signal(barrier, inc=1, device_id={"ra": (z + j) % n_ra}, device_id_type=MESH)
    for nb in (x_nb, y_nb):
        pl.semaphore_signal(barrier, inc=1, device_id={"cb": nb}, device_id_type=MESH)
    pl.semaphore_wait(barrier, n_ra + 1)

    xbuf[...] = tokens[...].astype(F32)
    gpre[0] = g_pre0[...].astype(F32)
    gpre[1] = g_pre1[...].astype(F32)
    gpost[0] = g_post0[...].astype(F32)
    gpost[1] = g_post1[...].astype(F32)

    def item(a):
        safe = jnp.maximum(a, 0)
        layer = safe // base
        r = safe % base
        g = r // n_k
        k = r % n_k
        ok = (a >= 0) & (r < per_layer) & (layer < 2)
        return ok, layer, g, k

    def remote(src, dst, send, recv, axis, to):
        return pltpu.make_async_remote_copy(
            src_ref=src, dst_ref=dst, send_sem=send, recv_sem=recv,
            device_id={axis: to}, device_id_type=MESH,
        )

    def p_copy(s, q, to):
        return remote(pslot.at[s, q], pslot.at[s, q], p_send.at[s, q], p_recv.at[s, q], "ra", to)

    def h_copy(s, q, to):
        return remote(hslot.at[s, q], hslot.at[s, q], h_send.at[s, q], h_recv.at[s, q], "ra", to)

    def a_copy(phase, part, j):
        src, dst = ((v1, r1), (v2, r2))[phase]
        to = (x_nb, y_nb)[(phase + j) % 2]
        i = 2 * phase + j
        return remote(src.at[part, j], dst.at[part, j], a_send.at[part, i], a_recv.at[part, i], "cb", to)

    def st_copy(part, src, j):
        to = (z + j) % n_ra
        return remote(stats.at[part, src], stats.at[part, src], st_send.at[part, j], st_recv.at[part, src], "ra", to)

    def ss_copy(part, src, to):
        return remote(sst.at[part, src], sst.at[part, src], ss_send.at[part], ss_recv.at[part, src], "ra", to)

    def row_stat(sq):
        lanes = sq[:, 0:128]
        for i in range(1, dl // 128):
            lanes = lanes + sq[:, 128 * i : 128 * (i + 1)]
        got = lax.dot_general(
            jnp.ones((8, 128), F32), lanes, (((1,), (1,)), ((), ())),
            precision=lax.Precision.HIGHEST, preferred_element_type=F32,
        )
        return jnp.concatenate([got] * (128 // part_rows), axis=1)

    def scale_of(ref, part):
        total = ref[part, 0]
        for i in range(1, n_ra):
            total = total + ref[part, i]
        mean = lax.dot_general(
            total[:, 0:part_rows], jnp.full((8, 128), 0.125, F32), (((0,), (0,)), ((), ())),
            precision=lax.Precision.HIGHEST, preferred_element_type=F32,
        )
        return lax.rsqrt(mean / depth + EPS)

    def wide(scale, n):
        return jnp.concatenate([scale] * (n // 128), axis=1)

    def tick(tau, carry):
        near = jnp.minimum(z, top - z)
        ok, layer, g, k = item(tau - LAG * near)

        @pl.when(ok & (g == 0))
        def _():
            i = layer * n_k + k
            pltpu.make_async_copy(gate0.at[:, pl.ds(0, SLICE)], wgu.at[i, :, pl.ds(0, SLICE)], w_sem.at[i, 0]).wait()
            pltpu.make_async_copy(up0.at[:, pl.ds(0, SLICE)], wgu.at[i, :, pl.ds(SLICE, SLICE)], w_sem.at[i, 1]).wait()

        ok, layer, g, k = item(tau - 2 * span + LAG * (top - near))

        @pl.when(ok & (g == 0))
        def _():
            i = layer * n_k + k
            pltpu.make_async_copy(down0.at[pl.ds(0, SLICE), :], wd.at[i], w_sem.at[i, 2]).wait()

        for s in (0, 1):
            p = z if s == 0 else top - z
            onward = z + 1 if s == 0 else z - 1
            backward = z - 1 if s == 0 else z + 1
            owner = top if s == 0 else 0

            a = tau - LAG * p
            safe = jnp.maximum(a, 0)
            layer = safe // base
            r = safe % base
            g = r // n_k
            k = r % n_k
            inside = (a >= 0) & (r < per_layer)
            rs = pl.ds(pl.multiple_of((2 * g + s) * part_rows, part_rows), part_rows)

            @pl.when(inside & (k == 0) & (layer >= 1) & (layer <= 2))
            def _():
                part = ((layer - 1) * GROUPS + g) * 2 + s
                for j in range(1, n_ra):
                    st_copy(part, (z + j) % n_ra, j).wait_recv()
                scale = wide(scale_of(stats, part), dl)
                x1 = xbuf[rs, :] + 0.5 * branch[rs, :].astype(F32) * scale * gpost[layer - 1]
                xbuf[rs, :] = x1

            @pl.when(inside & (k == 0) & (layer < 2))
            def _():
                part = (layer * GROUPS + g) * 2 + s
                x = xbuf[rs, :]
                ybuf[rs, :] = (x * gpre[layer]).astype(BF16)
                sst[part, p] = row_stat(x * x)

                @pl.when(p < top)
                def _():
                    ss_copy(part, p, owner).start()

                @pl.when(p == top)
                def _():
                    for j in range(top):
                        ss_copy(part, j, owner).wait_recv()
                    rss[s] = scale_of(sst, part)

            @pl.when(inside & (layer < 2))
            def _():
                i = layer * n_k + k
                q = layer * per_layer + r
                pbuf[...] = dot(ybuf[rs, :], wgu[i])

                @pl.when(p > 0)
                def _():
                    p_copy(s, q, onward).wait_recv()

                @pl.when(p == 0)
                def _():
                    pslot[s, q] = pbuf[...].astype(BF16)
                    p_copy(s, q, onward).start()

                @pl.when((p > 0) & (p < top))
                def _():
                    pslot[s, q] = (pbuf[...] + pslot[s, q].astype(F32)).astype(BF16)
                    p_copy(s, q, onward).start()

                @pl.when(p == top)
                def _():
                    full = (pbuf[...] + pslot[s, q].astype(F32)) * wide(rss[s], 2 * SLICE)
                    gate = full[:, :SLICE]
                    hslot[s, q] = (gate / (1.0 + jnp.exp(-gate)) * full[:, SLICE:]).astype(BF16)
                    h_copy(s, q, backward).start()

            b = tau - 2 * span + LAG * p
            ok, layer, g, k = item(b)

            @pl.when(ok)
            def _():
                i = layer * n_k + k
                q = (layer * GROUPS + g) * n_k + k
                rs = pl.ds(pl.multiple_of((2 * g + s) * part_rows, part_rows), part_rows)

                @pl.when(p < top)
                def _():
                    h_copy(s, q, backward).wait_recv()

                @pl.when((p < top) & (p > 0))
                def _():
                    h_copy(s, q, backward).start()

                @pl.when(k == 0)
                def _():
                    acc[rs, :] = dot(hslot[s, q], wd[i])

                @pl.when(k > 0)
                def _():
                    acc[rs, :] += dot(hslot[s, q], wd[i])

                @pl.when(k == n_k - 1)
                def _():
                    part = (layer * GROUPS + g) * 2 + s
                    for j in range(2):
                        v1[part, j] = acc[rs, half * j : half * (j + 1)].astype(BF16)
                        a_copy(0, part, j).start()

            ok, layer, g, k = item(b - LAG)

            @pl.when(ok & (k == n_k - 1))
            def _():
                part = (layer * GROUPS + g) * 2 + s
                for j in range(2):
                    a_copy(0, part, j).wait_recv()
                    v2[part, j] = (v1[part, j].astype(F32) + r1[part, j].astype(F32)).astype(BF16)
                    a_copy(1, part, j).start()

            ok, layer, g, k = item(b - 2 * LAG)

            @pl.when(ok & (k == n_k - 1))
            def _():
                part = (layer * GROUPS + g) * 2 + s
                rs = pl.ds(pl.multiple_of((2 * g + s) * part_rows, part_rows), part_rows)
                for j in range(2):
                    a_copy(1, part, j).wait_recv()
                    total = v2[part, j].astype(F32) + r2[part, j].astype(F32)
                    branch[rs, half * j : half * (j + 1)] = total.astype(BF16)
                value = branch[rs, :].astype(F32)
                stats[part, z] = row_stat(value * value)
                for j in range(1, n_ra):
                    st_copy(part, z, j).start()

        return carry

    last = 2 * base + (GROUPS - 1) * n_k + span + 1
    lax.fori_loop(0, last, tick, 0)

    out[...] = xbuf[...]

    def finish(q, carry):
        for s in (0, 1):
            p = z if s == 0 else top - z

            @pl.when(p < top)
            def _():
                p_copy(s, q, z).wait_send()

            @pl.when(p > 0)
            def _():
                h_copy(s, q, z).wait_send()

        return carry

    lax.fori_loop(0, 2 * per_layer, finish, 0)

    def finish_parts(part, carry):
        for phase in range(2):
            for j in range(2):
                a_copy(phase, part, j).wait_send()
        for j in range(1, n_ra):
            st_copy(part, z, j).wait_send()
        s = part % 2
        p = jnp.where(s == 0, z, top - z)

        @pl.when(p < top)
        def _():
            ss_copy(part, p, z).wait_send()

        return carry

    lax.fori_loop(0, 4 * GROUPS, finish_parts, 0)


def shards(n_ra, tokens, g_pre0, gate0, up0, down0, g_post0, g_pre1, gate1, up1, down1, g_post1):
    rows, dl = tokens.shape
    n_k = gate0.shape[1] // SLICE
    parts = 4 * GROUPS
    items = 2 * GROUPS * n_k
    pr = rows // (2 * GROUPS)
    vmem = pl.BlockSpec(memory_space=pltpu.VMEM)
    hbm = pl.BlockSpec(memory_space=pl.ANY)
    dma = pltpu.SemaphoreType.DMA
    row = lambda g: g.reshape(1, dl)
    return pl.pallas_call(
        functools.partial(kernel, n_ra),
        out_shape=jax.ShapeDtypeStruct((rows, dl), F32),
        in_specs=[vmem, vmem, hbm, hbm, hbm, vmem, vmem, hbm, hbm, hbm, vmem],
        out_specs=vmem,
        scratch_shapes=[
            pltpu.VMEM((2 * n_k, dl, 2 * SLICE), BF16),
            pltpu.VMEM((2 * n_k, SLICE, dl), BF16),
            pltpu.VMEM((2, items, pr, 2 * SLICE), BF16),
            pltpu.VMEM((2, items, pr, SLICE), BF16),
            pltpu.VMEM((pr, 2 * SLICE), F32),
            pltpu.VMEM((rows, dl), F32),
            pltpu.VMEM((rows, dl), BF16),
            pltpu.VMEM((rows, dl), F32),
            pltpu.VMEM((rows, dl), BF16),
            pltpu.VMEM((parts, 2, pr, dl // 2), BF16),
            pltpu.VMEM((parts, 2, pr, dl // 2), BF16),
            pltpu.VMEM((parts, 2, pr, dl // 2), BF16),
            pltpu.VMEM((parts, 2, pr, dl // 2), BF16),
            pltpu.VMEM((parts, n_ra, 8, 128), F32),
            pltpu.VMEM((parts, n_ra, 8, 128), F32),
            pltpu.VMEM((2, pr, 128), F32),
            pltpu.VMEM((2, 1, dl), F32),
            pltpu.VMEM((2, 1, dl), F32),
            dma((2 * n_k, 3)),
            dma((2, items)),
            dma((2, items)),
            dma((2, items)),
            dma((2, items)),
            dma((parts, 4)),
            dma((parts, 4)),
            dma((parts, n_ra)),
            dma((parts, n_ra)),
            dma((parts,)),
            dma((parts, n_ra)),
        ],
        compiler_params=pltpu.CompilerParams(
            collective_id=0, has_side_effects=True, vmem_limit_bytes=67043328
        ),
    )(
        tokens, row(g_pre0), gate0, up0, down0, row(g_post0),
        row(g_pre1), gate1, up1, down1, row(g_post1),
    )


def solution(mesh):
    placed = (
        P("dp", "ra"),
        P("ra"),
        P("ra", "cb"),
        P("ra", "cb"),
        P("cb", "ra"),
        P("ra"),
        P("ra"),
        P("ra", "cb"),
        P("ra", "cb"),
        P("cb", "ra"),
        P("ra"),
    )
    return jax.shard_map(
        functools.partial(shards, mesh.shape["ra"]),
        mesh=mesh, in_specs=placed, out_specs=P("dp", "ra"), check_vma=False,
    )
```

time: 384 us -> 153 us (0.40)
  waiting for transfers between devices: 278 us -> 0 us
  Pallas kernels: 0 us -> 145 us
  blocking collectives: 45.2 us -> 0 us
  matrix products: 33.6 us -> 0 us
  between operations: 13.6 us -> 0.01 us
  other arithmetic: 12.4 us -> 0 us
  local copies, waits for them, and re-layouts: 0.03 us -> 7.4 us
    pallas_call x0 -> x1, Pallas kernels: none -> 145 us  [shards(): pl.pallas_call(functools.partial(kernel, n_ra), out_shape=jax.ShapeDtypeS...]
    reduce_scatter x4 -> x0, waiting for transfers between devices: 122 us -> none  [the longest x2 68.9 us: project(): lax.psum_scatter(up_part.astype(jnp.bfloat16), 'ra', scatter_dimension=0,...]
    psum x2 -> x0, waiting for transfers between devices: 88.9 us -> none  [project(): total = lax.psum(partial_value.astype(jnp.bfloat16), 'cb')]
    all_gather x2 -> x0, waiting for transfers between devices: 67.2 us -> none  [project(): hidden = lax.all_gather(share, 'ra', axis=0, tiled=True)]
    psum x4 -> x0, blocking collectives: 45.2 us -> none  [the longest x2 23.4 us: branch_squares(): return lax.psum(jnp.sum(branch * branch, axis=1, keepdims=True), 'ra')]
    dot_general x6 -> x0, matrix products: 33.6 us -> none  [the longest x2 11.5 us: project(): gate_part = jnp.dot(normed, gate_weight, preferred_element_type=jnp.float32)]
    reduce_sum x4 -> x0, other arithmetic: 5.18 us -> none  [the longest x2 2.73 us: stream_squares(): return lax.psum(jnp.sum(stream * stream, axis=1, keepdims=True), 'ra')]
    reshape x0 -> x4, local copies, waits for them, and re-layouts: none -> 5.1 us  [shards(): row = lambda g: g.reshape(1, dl)]
  transfers between devices with their start and end apart: 8 -> 0, of which waited for: 8 -> 0; matrix products, arithmetic and copies ran while one was open for 3% -> 0% of each run, Pallas kernels for 0% -> 0%
where the time goes in v1:
time: 153 us
  Pallas kernels  145 us (95%)
  local copies, waits for them, and re-layouts  7.4 us (5%)
    pallas_call x1, Pallas kernels, shards(): pl.pallas_call(functools.partial(kernel, n_ra), out_shape=jax.ShapeDtypeS...  145 us
    reshape x4, local copies, waits for them, and re-layouts, shards(): row = lambda g: g.reshape(1, dl)  5.1 us

profile of v1, /device:TPU:0, one launch (start us, length us, event | category | flops | bytes accessed | tf_op | source)
XLA Modules:
  0.0 152.9 jit_solution(16874913427533322089)
XLA Ops:
  0.0 1.3 reshape.12.g_pre0
  1.3 1.3 reshape.13.g_post0
  2.6 1.3 reshape.14.g_pre1
  3.8 1.3 reshape.15.g_post1
  5.1 145.5 %shard_map.109 = f32[256,1024]{1,0:T(8,128)} custom-call(bf16[256,1024]{1,0:T(8,128)(2,1)} %tokens.1, bf16[1,1024]{1,0:T(2,128)(2,1)} %reshape.12.g_pre0, bf16[1024,2816]{1,0:T(8,128)(2,1)} %gate0.1, bf16[1024,2816]{1,0:T(8,128)(2,1)} %up0.1, bf16[2816,1024]{1,0:T(8,128)(2,1)} %down0.1, bf16[1,1024]{1,0:T(2,128)(2,1)} %reshape.13.g_post0, ...), custom_call_target="tpu_custom_call" | custom-call | tf_op jit(solution)/shard_map/pallas_call | solution.py:323
  150.6 2.3 %copy.13 = f32[256,1024]{1,0:T(8,128)} copy(f32[256,1024]{1,0:T(8,128)} %shard_map.109) | data formatting | bytes 2097152

commit v2 on v1

v2 whole, which is shorter than its diff:
```python
import functools

import jax
import jax.numpy as jnp
from jax import lax
from jax.experimental import pallas as pl
from jax.experimental.pallas import tpu as pltpu
from jax.sharding import PartitionSpec as P

EPS = 1e-06
MESH = pl.DeviceIdType.MESH
F32 = jnp.float32
BF16 = jnp.bfloat16
GROUPS = 2
SLICE = 256
LAG = 2
XLAG = 2


def dot(a, b):
    return jnp.dot(a, b, preferred_element_type=F32)


def kernel(
    n_ra, tokens, g_pre0, gate0, up0, down0, g_post0, g_pre1, gate1, up1, down1, g_post1,
    out, wgu, wd, pslot, hslot, gbuf, xbuf, ybuf, acc, branch, v1, r1, v2, r2,
    stats, sst, rss, gpre, gpost,
    w_sem, p_send, p_recv, h_send, h_recv, a_send, a_recv, st_send, st_recv, ss_send, ss_recv,
):
    rows, dl = xbuf.shape
    depth = dl * n_ra
    n_k = gate0.shape[1] // SLICE
    group_rows = rows // GROUPS
    part_rows = group_rows // 2
    per_layer = GROUPS * n_k
    top = n_ra - 1
    span = LAG * top
    ring = gbuf.shape[1]
    base = max(n_k + 2 * span + 3 * XLAG, per_layer)
    half = dl // 2

    z = lax.axis_index("ra")
    c = lax.axis_index("cb")
    x_nb = c + 1 - 2 * (c % 2)
    y_nb = c + 2 - 4 * (c // 2)
    near = jnp.minimum(z, top - z)

    for i in range(2 * n_k):
        layer, k = divmod(i, n_k)
        gate, up, down = ((gate0, up0, down0), (gate1, up1, down1))[layer]
        cols = pl.ds(k * SLICE, SLICE)
        pltpu.make_async_copy(gate.at[:, cols], wgu.at[i, :, pl.ds(0, SLICE)], w_sem.at[i, 0]).start()
        pltpu.make_async_copy(up.at[:, cols], wgu.at[i, :, pl.ds(SLICE, SLICE)], w_sem.at[i, 1]).start()
        pltpu.make_async_copy(down.at[cols, :], wd.at[i], w_sem.at[i, 2]).start()

    barrier = pltpu.get_barrier_semaphore()
    for j in range(1, n_ra):
        pl.semaphore_signal(barrier, inc=1, device_id={"ra": (z + j) % n_ra}, device_id_type=MESH)
    for nb in (x_nb, y_nb):
        pl.semaphore_signal(barrier, inc=1, device_id={"cb": nb}, device_id_type=MESH)

    xbuf[...] = tokens[...].astype(F32)
    gpre[0] = g_pre0[...].astype(F32)
    gpre[1] = g_pre1[...].astype(F32)
    gpost[0] = g_post0[...].astype(F32)
    gpost[1] = g_post1[...].astype(F32)
    pl.semaphore_wait(barrier, n_ra + 1)

    def item(a):
        safe = jnp.maximum(a, 0)
        layer = safe // base
        r = safe % base
        inside = (a >= 0) & (r < per_layer)
        return inside, layer, r // n_k, r % n_k

    def rows_of(g):
        return pl.ds(pl.multiple_of(g * group_rows, group_rows), group_rows)

    def remote(src, dst, send, recv, axis, to):
        return pltpu.make_async_remote_copy(
            src_ref=src, dst_ref=dst, send_sem=send, recv_sem=recv,
            device_id={axis: to}, device_id_type=MESH,
        )

    def p_copy(s, q, to):
        return remote(pslot.at[s, q], pslot.at[s, q], p_send.at[s, q], p_recv.at[s, q], "ra", to)

    def h_copy(s, q, to):
        return remote(hslot.at[q, s], hslot.at[q, s], h_send.at[s, q], h_recv.at[s, q], "ra", to)

    def a_copy(phase, part, j):
        src, dst = ((v1, r1), (v2, r2))[phase]
        to = (x_nb, y_nb)[(phase + j) % 2]
        i = 2 * phase + j
        return remote(src.at[part, j], dst.at[part, j], a_send.at[part, i], a_recv.at[part, i], "cb", to)

    def st_copy(part, src, j):
        to = (z + j) % n_ra
        return remote(stats.at[part, src], stats.at[part, src], st_send.at[part, j], st_recv.at[part, src], "ra", to)

    def ss_copy(part, src, e):
        to = (0, top)[e]
        return remote(sst.at[part, src], sst.at[part, src], ss_send.at[part, e], ss_recv.at[part, src], "ra", to)

    def row_stat(sq):
        lanes = sq[:, 0:128]
        for i in range(1, dl // 128):
            lanes = lanes + sq[:, 128 * i : 128 * (i + 1)]
        got = lax.dot_general(
            jnp.ones((8, 128), F32), lanes, (((1,), (1,)), ((), ())),
            precision=lax.Precision.HIGHEST, preferred_element_type=F32,
        )
        return jnp.concatenate([got] * (128 // group_rows), axis=1)

    def scale_of(ref, part):
        total = ref[part, 0]
        for i in range(1, n_ra):
            total = total + ref[part, i]
        mean = lax.dot_general(
            total[:, 0:group_rows], jnp.full((8, 128), 0.125, F32), (((0,), (0,)), ((), ())),
            precision=lax.Precision.HIGHEST, preferred_element_type=F32,
        )
        return lax.rsqrt(mean / depth + EPS)

    def wide(scale, n):
        return jnp.concatenate([scale] * (n // 128), axis=1)

    def tick(tau, carry):
        inside, layer, g, k = item(tau - LAG * near)

        @pl.when(inside & (k == 0) & (layer >= 1) & (layer <= 2))
        def _():
            part = (layer - 1) * GROUPS + g
            rs = rows_of(g)
            for j in range(1, n_ra):
                st_copy(part, (z + j) % n_ra, j).wait_recv()
            scale = wide(scale_of(stats, part), dl)
            x1 = xbuf[rs, :] + 0.5 * branch[rs, :].astype(F32) * scale * gpost[layer - 1]
            xbuf[rs, :] = x1

        @pl.when(inside & (k == 0) & (layer < 2))
        def _():
            part = layer * GROUPS + g
            rs = rows_of(g)
            x = xbuf[rs, :]
            ybuf[rs, :] = (x * gpre[layer]).astype(BF16)
            sst[part, z] = row_stat(x * x)

            for e in (0, 1):
                @pl.when(z != (0, top)[e])
                def _():
                    ss_copy(part, z, e).start()

        @pl.when(inside & (g == 0) & (layer < 2))
        def _():
            i = layer * n_k + k
            pltpu.make_async_copy(gate0.at[:, pl.ds(0, SLICE)], wgu.at[i, :, pl.ds(0, SLICE)], w_sem.at[i, 0]).wait()
            pltpu.make_async_copy(up0.at[:, pl.ds(0, SLICE)], wgu.at[i, :, pl.ds(SLICE, SLICE)], w_sem.at[i, 1]).wait()

        @pl.when(inside & (layer < 2))
        def _():
            slot = ((layer * GROUPS + g) * n_k + k) % ring
            got = dot(ybuf[rows_of(g), :], wgu[layer * n_k + k])
            gbuf[0, slot] = got[:part_rows]
            gbuf[1, slot] = got[part_rows:]

        for s in (0, 1):
            p = z if s == 0 else top - z
            onward = z + 1 if s == 0 else z - 1
            backward = z - 1 if s == 0 else z + 1

            inside, layer, g, k = item(tau - LAG * p)
            ok = inside & (layer < 2)
            q = (layer * GROUPS + g) * n_k + k

            @pl.when(ok & (p == 0))
            def _():
                pslot[s, q] = gbuf[s, q % ring].astype(BF16)
                p_copy(s, q, onward).start()

            @pl.when(ok & (p > 0) & (p < top))
            def _():
                p_copy(s, q, onward).wait_recv()
                pslot[s, q] = (gbuf[s, q % ring] + pslot[s, q].astype(F32)).astype(BF16)
                p_copy(s, q, onward).start()

            @pl.when(ok & (p == top) & (k == 0))
            def _():
                part = layer * GROUPS + g
                for j in range(1, n_ra):
                    ss_copy(part, (z + j) % n_ra, 0).wait_recv()
                rss[...] = scale_of(sst, part)[part_rows * s : part_rows * (s + 1)]

            @pl.when(ok & (p == top))
            def _():
                p_copy(s, q, onward).wait_recv()
                full = (gbuf[s, q % ring] + pslot[s, q].astype(F32)) * wide(rss[...], 2 * SLICE)
                gate = full[:, :SLICE]
                hslot[q, s] = (gate / (1.0 + jnp.exp(-gate)) * full[:, SLICE:]).astype(BF16)
                h_copy(s, q, backward).start()

            inside, layer, g, k = item(tau - 2 * span + LAG * p)
            ok = inside & (layer < 2)
            q = (layer * GROUPS + g) * n_k + k

            @pl.when(ok & (p < top))
            def _():
                h_copy(s, q, backward).wait_recv()

            @pl.when(ok & (p < top) & (p > 0))
            def _():
                h_copy(s, q, backward).start()

        b = tau - 2 * span + LAG * near
        inside, layer, g, k = item(b)
        ok = inside & (layer < 2)

        @pl.when(ok & (g == 0))
        def _():
            pltpu.make_async_copy(down0.at[pl.ds(0, SLICE), :], wd.at[layer * n_k + k], w_sem.at[layer * n_k + k, 2]).wait()

        @pl.when(ok)
        def _():
            q = (layer * GROUPS + g) * n_k + k
            got = dot(hslot[q].reshape(group_rows, SLICE), wd[layer * n_k + k])

            @pl.when(k == 0)
            def _():
                acc[g] = got

            @pl.when(k > 0)
            def _():
                acc[g] += got

        @pl.when(ok & (k == n_k - 1))
        def _():
            part = layer * GROUPS + g
            for j in range(2):
                v1[part, j] = acc[g, :, half * j : half * (j + 1)].astype(BF16)
                a_copy(0, part, j).start()

        inside, layer, g, k = item(b - XLAG)

        @pl.when(inside & (layer < 2) & (k == n_k - 1))
        def _():
            part = layer * GROUPS + g
            for j in range(2):
                a_copy(0, part, j).wait_recv()
                v2[part, j] = (v1[part, j].astype(F32) + r1[part, j].astype(F32)).astype(BF16)
                a_copy(1, part, j).start()

        inside, layer, g, k = item(b - 2 * XLAG)

        @pl.when(inside & (layer < 2) & (k == n_k - 1))
        def _():
            part = layer * GROUPS + g
            rs = rows_of(g)
            for j in range(2):
                a_copy(1, part, j).wait_recv()
                total = v2[part, j].astype(F32) + r2[part, j].astype(F32)
                branch[rs, half * j : half * (j + 1)] = total.astype(BF16)
            value = branch[rs, :].astype(F32)
            stats[part, z] = row_stat(value * value)
            for j in range(1, n_ra):
                st_copy(part, z, j).start()

        return carry

    last = 2 * base + (GROUPS - 1) * n_k + LAG * (top // 2) + 1
    lax.fori_loop(0, last, tick, 0)

    out[...] = xbuf[...]

    def finish(q, carry):
        for s in (0, 1):
            p = z if s == 0 else top - z

            @pl.when(p < top)
            def _():
                p_copy(s, q, z).wait_send()

            @pl.when(p > 0)
            def _():
                h_copy(s, q, z).wait_send()

        return carry

    lax.fori_loop(0, 2 * per_layer, finish, 0)

    def finish_parts(part, carry):
        for phase in range(2):
            for j in range(2):
                a_copy(phase, part, j).wait_send()
        for j in range(1, n_ra):
            st_copy(part, z, j).wait_send()
        for e in (0, 1):
            @pl.when(z != (0, top)[e])
            def _():
                ss_copy(part, z, e).wait_send()

        return carry

    lax.fori_loop(0, 2 * GROUPS, finish_parts, 0)


def shards(n_ra, tokens, g_pre0, gate0, up0, down0, g_post0, g_pre1, gate1, up1, down1, g_post1):
    rows, dl = tokens.shape
    n_k = gate0.shape[1] // SLICE
    parts = 2 * GROUPS
    items = 2 * GROUPS * n_k
    gr = rows // GROUPS
    pr = gr // 2
    vmem = pl.BlockSpec(memory_space=pltpu.VMEM)
    hbm = pl.BlockSpec(memory_space=pl.ANY)
    dma = pltpu.SemaphoreType.DMA
    row = lambda g: g.reshape(1, dl)
    return pl.pallas_call(
        functools.partial(kernel, n_ra),
        out_shape=jax.ShapeDtypeStruct((rows, dl), F32),
        in_specs=[vmem, vmem, hbm, hbm, hbm, vmem, vmem, hbm, hbm, hbm, vmem],
        out_specs=vmem,
        scratch_shapes=[
            pltpu.VMEM((2 * n_k, dl, 2 * SLICE), BF16),
            pltpu.VMEM((2 * n_k, SLICE, dl), BF16),
            pltpu.VMEM((2, items, pr, 2 * SLICE), BF16),
            pltpu.VMEM((items, 2, pr, SLICE), BF16),
            pltpu.VMEM((2, LAG * (n_ra - 1) + 1, pr, 2 * SLICE), F32),
            pltpu.VMEM((rows, dl), F32),
            pltpu.VMEM((rows, dl), BF16),
            pltpu.VMEM((GROUPS, gr, dl), F32),
            pltpu.VMEM((rows, dl), BF16),
            pltpu.VMEM((parts, 2, gr, dl // 2), BF16),
            pltpu.VMEM((parts, 2, gr, dl // 2), BF16),
            pltpu.VMEM((parts, 2, gr, dl // 2), BF16),
            pltpu.VMEM((parts, 2, gr, dl // 2), BF16),
            pltpu.VMEM((parts, n_ra, 8, 128), F32),
            pltpu.VMEM((parts, n_ra, 8, 128), F32),
            pltpu.VMEM((pr, 128), F32),
            pltpu.VMEM((2, 1, dl), F32),
            pltpu.VMEM((2, 1, dl), F32),
            dma((2 * n_k, 3)),
            dma((2, items)),
            dma((2, items)),
            dma((2, items)),
            dma((2, items)),
            dma((parts, 4)),
            dma((parts, 4)),
            dma((parts, n_ra)),
            dma((parts, n_ra)),
            dma((parts, 2)),
            dma((parts, n_ra)),
        ],
        compiler_params=pltpu.CompilerParams(
            collective_id=0, has_side_effects=True, vmem_limit_bytes=67043328
        ),
    )(
        tokens, row(g_pre0), gate0, up0, down0, row(g_post0),
        row(g_pre1), gate1, up1, down1, row(g_post1),
    )


def solution(mesh):
    placed = (
        P("dp", "ra"),
        P("ra"),
        P("ra", "cb"),
        P("ra", "cb"),
        P("cb", "ra"),
        P("ra"),
        P("ra"),
        P("ra", "cb"),
        P("ra", "cb"),
        P("cb", "ra"),
        P("ra"),
    )
    return jax.shard_map(
        functools.partial(shards, mesh.shape["ra"]),
        mesh=mesh, in_specs=placed, out_specs=P("dp", "ra"), check_vma=False,
    )
```

time: 153 us -> 157 us (1.026)
  Pallas kernels: 145 us -> 149 us
    pallas_call x1, Pallas kernels: 145 us -> 149 us  [shards(): pl.pallas_call(functools.partial(kernel, n_ra), out_shape=jax.ShapeDtypeS...]
where the time goes in v2:
time: 157 us; the launch traced here: 156 us
  Pallas kernels  149 us (95%)
  local copies, waits for them, and re-layouts  7.4 us (5%)
    pallas_call x1, Pallas kernels, shards(): pl.pallas_call(functools.partial(kernel, n_ra), out_shape=jax.ShapeDtypeS...  149 us
    reshape x4, local copies, waits for them, and re-layouts, shards(): row = lambda g: g.reshape(1, dl)  5.1 us

profile of v2, /device:TPU:0, one launch (start us, length us, event | category | flops | bytes accessed | tf_op | source)
XLA Modules:
  0.0 156.2 jit_solution(15303020860405242279)
XLA Ops:
  0.0 1.3 reshape.12.g_pre0
  1.3 1.3 reshape.13.g_post0
  2.6 1.3 reshape.14.g_pre1
  3.8 1.3 reshape.15.g_post1
  5.1 148.8 %shard_map.109 = f32[256,1024]{1,0:T(8,128)} custom-call(bf16[256,1024]{1,0:T(8,128)(2,1)} %tokens.1, bf16[1,1024]{1,0:T(2,128)(2,1)} %reshape.12.g_pre0, bf16[1024,2816]{1,0:T(8,128)(2,1)} %gate0.1, bf16[1024,2816]{1,0:T(8,128)(2,1)} %up0.1, bf16[2816,1024]{1,0:T(8,128)(2,1)} %down0.1, bf16[1,1024]{1,0:T(2,128)(2,1)} %reshape.13.g_post0, ...), custom_call_target="tpu_custom_call" | custom-call | tf_op jit(solution)/shard_map/pallas_call | solution.py:317
  153.9 2.3 %copy.13 = f32[256,1024]{1,0:T(8,128)} copy(f32[256,1024]{1,0:T(8,128)} %shard_map.109) | data formatting | bytes 2097152

commit v3 on v2

--- a/solution.py
+++ b/solution.py
@@ -11,10 +11,10 @@
 MESH = pl.DeviceIdType.MESH
 F32 = jnp.float32
 BF16 = jnp.bfloat16
-GROUPS = 2
+GROUPS = 4
 SLICE = 256
-LAG = 2
-XLAG = 2
+LAG = 4
+XLAG = 5
 
 
 def dot(a, b):

time: 157 us -> 151 us (0.962)
  Pallas kernels: 149 us -> 143 us
    pallas_call x1, Pallas kernels: 149 us -> 143 us  [shards(): pl.pallas_call(functools.partial(kernel, n_ra), out_shape=jax.ShapeDtypeS...]
where the time goes in v3:
time: 151 us
  Pallas kernels  143 us (95%)
  local copies, waits for them, and re-layouts  7.4 us (5%)
    pallas_call x1, Pallas kernels, shards(): pl.pallas_call(functools.partial(kernel, n_ra), out_shape=jax.ShapeDtypeS...  143 us
    reshape x4, local copies, waits for them, and re-layouts, shards(): row = lambda g: g.reshape(1, dl)  5.1 us

profile of v3, /device:TPU:0, one launch (start us, length us, event | category | flops | bytes accessed | tf_op | source)
XLA Modules:
  0.0 150.6 jit_solution(2582215078817252453)
XLA Ops:
  0.0 1.3 reshape.12.g_pre0
  1.3 1.3 reshape.13.g_post0
  2.6 1.3 reshape.14.g_pre1
  3.8 1.3 reshape.15.g_post1
  5.1 143.2 %shard_map.109 = f32[256,1024]{1,0:T(8,128)} custom-call(bf16[256,1024]{1,0:T(8,128)(2,1)} %tokens.1, bf16[1,1024]{1,0:T(2,128)(2,1)} %reshape.12.g_pre0, bf16[1024,2816]{1,0:T(8,128)(2,1)} %gate0.1, bf16[1024,2816]{1,0:T(8,128)(2,1)} %up0.1, bf16[2816,1024]{1,0:T(8,128)(2,1)} %down0.1, bf16[1,1024]{1,0:T(2,128)(2,1)} %reshape.13.g_post0, ...), custom_call_target="tpu_custom_call" | custom-call | tf_op jit(solution)/shard_map/pallas_call | solution.py:317
  148.3 2.3 %copy.13 = f32[256,1024]{1,0:T(8,128)} copy(f32[256,1024]{1,0:T(8,128)} %shard_map.109) | data formatting | bytes 2097152
